TPU v7x, 32 devices: a whole 2x2x4 slice. The times are simulated.
32 devices in a mesh: fs: 8 (over z, x), tp: 4 (over y, core).
Axes of the slice: x: 2, y: 2, z: 4, core: 2. Of those that a mesh axis runs over, the one named last changes fastest.
Arguments:
- tokens: bfloat16 [4096, 2048], P('fs', 'tp'), may hold values from -6 to 6
- pre_gain: float32 [2048], replicated, may hold values from 0.1 to 1.9
- pre_gate: float32 [2048, 2816], P('fs', 'tp'), may hold values from -0.125 to 0.125
- pre_up: float32 [2048, 2816], P('fs', 'tp'), may hold values from -0.125 to 0.125
- pre_down: float32 [2816, 2048], P('fs', 'tp'), may hold values from -0.109375 to 0.109375
- mix_gain: float32 [2048], replicated, may hold values from 0.1 to 1.9
- branch_proj: float32 [2048, 1024], P('fs', 'tp'), may hold values from -0.125 to 0.125
- gate_proj: float32 [2048, 1024], P('fs', 'tp'), may hold values from -0.125 to 0.125
- conv_taps: float32 [4, 1024], P(None, 'tp'), may hold values from -3 to 3
- retain_blocks: float32 [16, 64, 64], P('tp'), may hold values from -0.75 to 0.75
- admit_blocks: float32 [16, 64, 64], P('tp'), may hold values from -0.75 to 0.75
- decay_param: float32 [1024], P('tp'), may hold values from 5 to 8.5
- channel_gain: float32 [1024], replicated, may hold values from 0.1 to 1.9
- out_proj: float32 [1024, 2048], P('fs', 'tp'), may hold values from -0.1875 to 0.1875
- post_gain: float32 [2048], replicated, may hold values from 0.1 to 1.9
- post_gate: float32 [2048, 2816], P('fs', 'tp'), may hold values from -0.125 to 0.125
- post_up: float32 [2048, 2816], P('fs', 'tp'), may hold values from -0.125 to 0.125
- post_down: float32 [2816, 2048], P('fs', 'tp'), may hold values from -0.109375 to 0.109375
Outputs:
- layer_out: bfloat16 [4096, 2048], P('fs', 'tp')
All inputs are finite; a program needn't handle non-finite values.
Results may differ from a plain program's by a relative error of at most 0.012.
Values may be sent and summed in bfloat16 or wider, within the bound.
A program may use at most 64 MiB of HBM per device.

v0:
```python
import jax
import jax.numpy as jnp
from jax import lax
from jax.sharding import PartitionSpec as P

SEQ_LEN = 128
EPSILON = 1e-06
DECAY_SCALE = 8.0


def normalize(values, norm_gain):
    floats = values.astype(jnp.float32)
    scaled = floats * lax.rsqrt(jnp.mean(floats * floats, axis=-1, keepdims=True) + EPSILON)
    return (scaled * norm_gain).astype(jnp.bfloat16)


def combine(earlier, latter):
    keep_early, add_early = earlier
    keep_late, add_late = latter
    return (keep_early * keep_late, keep_late * add_early + add_late)


def widen(residual):
    return lax.all_gather(residual, "tp", axis=1, tiled=True)


def contract(operand, stacked):
    return jnp.dot(
        operand,
        lax.all_gather(stacked.astype(jnp.bfloat16), "fs", axis=0, tiled=True),
        preferred_element_type=jnp.float32,
    )


def feed_forward(residual, norm_gain, gate_matrix, up_matrix, down_matrix):
    normed = normalize(widen(residual), norm_gain)
    products = contract(normed, jnp.concatenate((gate_matrix, up_matrix), axis=1))
    split_at = gate_matrix.shape[1]
    hidden = (jax.nn.silu(products[:, :split_at]) * products[:, split_at:]).astype(jnp.bfloat16)
    all_hidden = lax.all_gather(hidden, "tp", axis=1, tiled=True)
    return (residual.astype(jnp.float32) + 0.5 * contract(all_hidden, down_matrix)).astype(
        jnp.bfloat16
    )


def block_gate(convolved, blocks):
    grouped = convolved.reshape(
        convolved.shape[0], convolved.shape[1], blocks.shape[0], blocks.shape[1]
    )
    mixed = jnp.einsum(
        "sthi,hij->sthj", grouped, blocks.astype(jnp.bfloat16), preferred_element_type=jnp.float32
    )
    return jax.nn.sigmoid(mixed).reshape(convolved.shape)


def recurrent_mixer(
    residual,
    norm_gain,
    branch_matrix,
    gate_matrix,
    conv_taps,
    retain_blocks,
    admit_blocks,
    decay_param,
    channel_gain,
    out_matrix,
):
    normed = normalize(widen(residual), norm_gain)
    products = contract(normed, jnp.concatenate((branch_matrix, gate_matrix), axis=1))
    local_width = branch_matrix.shape[1]
    branch = products[:, :local_width]
    gate_act = products[:, local_width:]
    taps_count = conv_taps.shape[0]
    sequences = residual.shape[0] // SEQ_LEN
    framed = branch.reshape(sequences, SEQ_LEN, local_width)
    padded = jnp.pad(framed, ((0, 0), (taps_count - 1, 0), (0, 0)))
    convolved = jnp.zeros_like(framed)
    for tap_index in range(taps_count):
        convolved = convolved + padded[:, tap_index : tap_index + SEQ_LEN] * conv_taps[tap_index]
    convolved = convolved.astype(jnp.bfloat16)
    retained = block_gate(convolved, retain_blocks)
    admitted = block_gate(convolved, admit_blocks)
    log_keep = -DECAY_SCALE * retained * jax.nn.softplus(-decay_param)
    inject = jnp.sqrt(-jnp.expm1(2.0 * log_keep)) * admitted * convolved.astype(jnp.float32)
    _, states = lax.associative_scan(combine, (jnp.exp(log_keep), inject), axis=1)
    mixed_rows = (states.reshape(residual.shape[0], local_width) * jax.nn.gelu(gate_act)).astype(
        jnp.bfloat16
    )
    all_channels = lax.all_gather(mixed_rows, "tp", axis=1, tiled=True)
    mixed_normed = normalize(all_channels, channel_gain)
    return (residual.astype(jnp.float32) + contract(mixed_normed, out_matrix)).astype(jnp.bfloat16)


def local(
    tokens,
    pre_gain,
    pre_gate,
    pre_up,
    pre_down,
    mix_gain,
    branch_proj,
    gate_proj,
    conv_taps,
    retain_blocks,
    admit_blocks,
    decay_param,
    channel_gain,
    out_proj,
    post_gain,
    post_gate,
    post_up,
    post_down,
):
    after_pre = feed_forward(tokens, pre_gain, pre_gate, pre_up, pre_down)
    after_mix = recurrent_mixer(
        after_pre,
        mix_gain,
        branch_proj,
        gate_proj,
        conv_taps,
        retain_blocks,
        admit_blocks,
        decay_param,
        channel_gain,
        out_proj,
    )
    return feed_forward(after_mix, post_gain, post_gate, post_up, post_down)


def solution(mesh):
    placed = (
        P("fs", "tp"),
        P(),
        P("fs", "tp"),
        P("fs", "tp"),
        P("fs", "tp"),
        P(),
        P("fs", "tp"),
        P("fs", "tp"),
        P(None, "tp"),
        P("tp", None, None),
        P("tp", None, None),
        P("tp"),
        P(),
        P("fs", "tp"),
        P(),
        P("fs", "tp"),
        P("fs", "tp"),
        P("fs", "tp"),
    )
    return jax.shard_map(
        local, mesh=mesh, in_specs=placed, out_specs=P("fs", "tp"), check_vma=False
    )
```

profile of v0, /device:TPU:0, one launch (start us, length us, event | category | flops | bytes accessed | tf_op | source)
XLA Modules:
  0.0 807.1 jit_solution(914277624177452306)
XLA Ops:
  10.4 23.8 %all-gather.13.cloned.1.call-done = bf16[512,2048]{1,0:T(8,128)(2,1)} async-done(((bf16[512,512]{1,0:T(8,128)(2,1)}), bf16[512,2048]{1,0:T(8,128)(2,1)}) %all-gather.13.cloned.1.call-update) | async-done | bytes 2097168 | tf_op jit(solution)/shard_map/all_gather | solution.py:24
  36.5 93.0 %all-gather.15.cloned.1.call-done = bf16[2048,1408]{0,1:T(8,128)(2,1)} async-done(((bf16[256,1408]{0,1:T(8,128)(2,1)}), bf16[2048,1408]{0,1:T(8,128)(2,1)}) %all-gather.15.cloned.1.call-update) | async-done | bytes 5767184 | tf_op jit(solution)/shard_map/all_gather | solution.py:30
  129.4 5.8 fusion.16
  137.0 50.1 %all-gather.19.cloned.1.call-done = bf16[2816,512]{1,0:T(8,128)(2,1)} async-done(((bf16[352,512]{1,0:T(8,128)(2,1)}), bf16[2816,512]{1,0:T(8,128)(2,1)}) %all-gather.19.cloned.1.call-update) | async-done | bytes 2883600 | tf_op jit(solution)/shard_map/all_gather | solution.py:30
  187.1 27.1 %all-gather.17.cloned.1.call-done = bf16[512,2816]{0,1:T(8,128)(2,1)} async-done(((bf16[512,704]{0,1:T(8,128)(2,1)}), bf16[512,2816]{0,1:T(8,128)(2,1)}) %all-gather.17.cloned.1.call-update) | async-done | bytes 2883600 | tf_op jit(solution)/shard_map/all_gather | solution.py:40
  214.2 5.2 fusion.29
  220.4 21.7 %all-gather.21.cloned.1.call-done = bf16[512,2048]{1,0:T(8,128)(2,1)} async-done(((bf16[512,512]{1,0:T(8,128)(2,1)}), bf16[512,2048]{1,0:T(8,128)(2,1)}) %all-gather.21.cloned.1.call-update) | async-done | bytes 2097168 | tf_op jit(solution)/shard_map/all_gather | solution.py:24
  244.4 48.9 %all-gather.23.cloned.1.call-done = bf16[2048,512]{1,0:T(8,128)(2,1)} async-done(((bf16[256,512]{1,0:T(8,128)(2,1)}), bf16[2048,512]{1,0:T(8,128)(2,1)}) %all-gather.23.cloned.1.call-update) | async-done | bytes 2097168 | tf_op jit(solution)/shard_map/all_gather | solution.py:30
  293.2 2.9 fusion.14
  299.5 9.1 %slice.212 = f32[4,64,256]{1,2,0:T(8,128)S(1)} slice(f32[4,128,256]{1,2,0:T(8,128)S(1)} %get-tuple-element.6), slice={[0:4:1], [0:127:2], [0:256:1]} | slice | bytes 524288 | tf_op jit(solution)/shard_map/slice | solution.py:85
  308.6 9.1 %slice.213 = f32[4,64,256]{1,2,0:T(8,128)S(1)} slice(f32[4,128,256]{1,2,0:T(8,128)S(1)} %get-tuple-element.6), slice={[0:4:1], [1:128:2], [0:256:1]} | slice | bytes 524288 | tf_op jit(solution)/shard_map/slice | solution.py:85
  317.6 9.1 %slice.211 = f32[4,64,256]{1,2,0:T(8,128)S(1)} slice(f32[4,128,256]{1,2,0:T(8,128)S(1)} %get-tuple-element.5), slice={[0:4:1], [1:128:2], [0:256:1]} | slice | bytes 524288 | tf_op jit(solution)/shard_map/slice | solution.py:85
  326.7 9.5 %slice.215 = f32[4,64,256]{1,2,0:T(8,128)} slice(f32[4,128,256]{1,2,0:T(8,128)S(1)} %get-tuple-element.5), slice={[0:4:1], [0:127:2], [0:256:1]} | slice | bytes 524288 | tf_op jit(solution)/shard_map/slice | solution.py:85
  337.4 4.6 slice.218
  342.0 4.7 slice.219
  346.7 5.3 slice.217
  352.1 5.2 slice.221
  361.0 3.2 slice.225
  364.2 3.4 slice.223
  367.6 3.1 slice.227
  396.6 3.4 slice.241
  400.0 3.3 slice.245
  408.7 3.5 slice.234
  414.0 3.7 slice.228
  420.0 3.1 slice.222
  423.1 3.1 slice.255
  426.2 6.1 slice.216
  432.2 5.2 slice.257
  437.4 9.5 %slice.259 = f32[4,63,256]{1,2,0:T(8,128)} slice(f32[4,128,256]{1,2,0:T(8,128)S(1)} %get-tuple-element.6), slice={[0:4:1], [2:128:2], [0:256:1]} | slice | bytes 516096 | tf_op jit(solution)/shard_map/slice | solution.py:85
  446.9 9.9 %slice.210 = f32[4,63,256]{1,2,0:T(8,128)} slice(f32[4,128,256]{1,2,0:T(8,128)S(1)} %copy-done.1), slice={[0:4:1], [2:128:2], [0:256:1]} | slice | bytes 516096 | tf_op jit(solution)/shard_map/slice | solution.py:85
  463.8 4.3 pad.51
  470.0 2.5 pad.53
  487.7 2.9 pad.55
  491.5 3.7 pad.57
  497.5 3.6 pad.56
  502.3 4.5 pad.58
  506.8 4.6 pad.59
  512.3 9.8 %pad.61 = f32[4,128,256]{1,2,0:T(8,128)S(1)} pad(f32[4,64,256]{1,2,0:T(8,128)} %add.195, f32[]{:T(128)} %constant.10.clone.1), padding=0_0_0x1_0_1x0_0_0 | pad | bytes 786436 | tf_op jit(solution)/shard_map/pad | solution.py:85
  522.5 8.8 %pad.60 = f32[4,128,256]{1,2,0:T(8,128)S(1)} pad(f32[4,64,256]{1,2,0:T(8,128)S(1)} %pad_maximum_fusion.4, f32[]{:T(128)} %constant.10.clone.1), padding=0_0_0x0_1_1x0_0_0 | pad | bytes 786436 | tf_op jit(solution)/shard_map/pad | solution.py:85
  533.3 14.7 %all-gather.25.cloned.1.call-done = bf16[512,1024]{1,0:T(8,128)(2,1)} async-done(((bf16[512,256]{1,0:T(8,128)(2,1)}), bf16[512,1024]{1,0:T(8,128)(2,1)}) %all-gather.25.cloned.1.call-update) | async-done | bytes 1048592 | tf_op jit(solution)/shard_map/all_gather | solution.py:89
  549.6 40.9 %all-gather.27.cloned.1.call-done = bf16[1024,512]{1,0:T(8,128)(2,1)} async-done(((bf16[128,512]{1,0:T(8,128)(2,1)}), bf16[1024,512]{1,0:T(8,128)(2,1)}) %all-gather.27.cloned.1.call-update) | async-done | bytes 1048592 | tf_op jit(solution)/shard_map/all_gather | solution.py:30
  590.5 3.1 fusion.30
  595.8 19.2 %all-gather.29.cloned.1.call-done = bf16[512,2048]{1,0:T(8,128)(2,1)} async-done(((bf16[512,512]{1,0:T(8,128)(2,1)}), bf16[512,2048]{1,0:T(8,128)(2,1)}) %all-gather.29.cloned.1.call-update) | async-done | bytes 2097168 | tf_op jit(solution)/shard_map/all_gather | solution.py:24
  617.3 92.8 %all-gather.31.cloned.1.call-done = bf16[2048,1408]{0,1:T(8,128)(2,1)} async-done(((bf16[256,1408]{0,1:T(8,128)(2,1)}), bf16[2048,1408]{0,1:T(8,128)(2,1)}) %all-gather.31.cloned.1.call-update) | async-done | bytes 5767184 | tf_op jit(solution)/shard_map/all_gather | solution.py:30
  710.1 5.8 fusion.12
  717.6 50.2 %all-gather.35.cloned.1.call-done = bf16[2816,512]{1,0:T(8,128)(2,1)} async-done(((bf16[352,512]{1,0:T(8,128)(2,1)}), bf16[2816,512]{1,0:T(8,128)(2,1)}) %all-gather.35.cloned.1.call-update) | async-done | bytes 2883600 | tf_op jit(solution)/shard_map/all_gather | solution.py:30
  767.8 27.1 %all-gather.33.cloned.1.call-done = bf16[512,2816]{0,1:T(8,128)(2,1)} async-done(((bf16[512,704]{0,1:T(8,128)(2,1)}), bf16[512,2816]{0,1:T(8,128)(2,1)}) %all-gather.33.cloned.1.call-update) | async-done | bytes 2883600 | tf_op jit(solution)/shard_map/all_gather | solution.py:40
  794.9 5.2 fusion.28
  (197 shorter events, 93.5 us)
Async XLA Ops:
  6.5 2.0 copy-start.21
  6.5 27.7 %all-gather.13.cloned.1.call-start = ((), (), s32[]{:S(2)}) async-start(), calls=%async_computation | async-start | bytes 2621440 | tf_op jit(solution)/shard_map/all_gather | solution.py:24
  7.3 2.3 copy-start.22
  7.3 122.1 %all-gather.15.cloned.1.call-start = ((), (), s32[]{:S(2)}) async-start(), calls=%async_computation.1 | async-start | bytes 6488064 | tf_op jit(solution)/shard_map/all_gather | solution.py:30
  9.5 119.9 %copy-start.36 = (f32[2048]{0:T(1024)S(1)}, f32[2048]{0:T(1024)}, u32[]{:S(2)}) copy-start(f32[2048]{0:T(1024)} %param.19) | copy-start | bytes 24580
  9.5 177.6 %all-gather.19.cloned.1.call-start = ((), (), s32[]{:S(2)}) async-start(), calls=%async_computation.3 | async-start | bytes 3244032 | tf_op jit(solution)/shard_map/all_gather | solution.py:30
  10.4 203.8 %all-gather.17.cloned.1.call-start = ((), (), s32[]{:S(2)}) async-start(), calls=%async_computation.2 | async-start | bytes 3604480 | tf_op jit(solution)/shard_map/all_gather | solution.py:40
  34.2 95.2 %copy-start.14 = (bf16[512,2048]{1,0:T(8,128)(2,1)S(1)}, bf16[512,2048]{1,0:T(8,128)(2,1)}, u32[]{:S(2)}) copy-start(bf16[512,2048]{1,0:T(8,128)(2,1)} %all-gather.13.cloned.1.call-done) | copy-start | bytes 6291460
  135.8 78.4 %copy-start.26 = (bf16[512,512]{1,0:T(8,128)(2,1)S(1)}, bf16[512,512]{1,0:T(8,128)(2,1)}, u32[]{:S(2)}) copy-start(bf16[512,512]{1,0:T(8,128)(2,1)} %param.18) | copy-start | bytes 1572868
  136.9 82.5 %copy-start.29 = (f32[256,256]{1,0:T(8,128)S(1)}, f32[256,256]{1,0:T(8,128)}, u32[]{:S(2)}) copy-start(f32[256,256]{1,0:T(8,128)} %param.24) | copy-start | bytes 786436
  137.0 82.5 %copy-start.30 = (f32[256,256]{1,0:T(8,128)S(1)}, f32[256,256]{1,0:T(8,128)}, u32[]{:S(2)}) copy-start(f32[256,256]{1,0:T(8,128)} %param.25) | copy-start | bytes 786436
  137.0 105.2 %all-gather.21.cloned.1.call-start = ((), (), s32[]{:S(2)}) async-start(), calls=%async_computation.4 | async-start | bytes 2621440 | tf_op jit(solution)/shard_map/all_gather | solution.py:24
  219.4 73.8 %copy-start.37 = (f32[2048]{0:T(1024)S(1)}, f32[2048]{0:T(1024)}, u32[]{:S(2)}) copy-start(f32[2048]{0:T(1024)} %param.23) | copy-start | bytes 24580
  219.4 73.8 %all-gather.23.cloned.1.call-start = ((), (), s32[]{:S(2)}) async-start(), calls=%async_computation.5 | async-start | bytes 2359296 | tf_op jit(solution)/shard_map/all_gather | solution.py:30
  220.3 327.7 %all-gather.25.cloned.1.call-start = ((), (), s32[]{:S(2)}) async-start(), calls=%async_computation.6 | async-start | bytes 1310720 | tf_op jit(solution)/shard_map/all_gather | solution.py:89
  242.1 51.1 %copy-start.16 = (bf16[512,2048]{1,0:T(8,128)(2,1)S(1)}, bf16[512,2048]{1,0:T(8,128)(2,1)}, u32[]{:S(2)}) copy-start(bf16[512,2048]{1,0:T(8,128)(2,1)} %all-gather.21.cloned.1.call-done) | copy-start | bytes 6291460
  296.1 1.8 copy-start.34
  299.4 27.2 %copy-start = (f32[4,128,256]{1,2,0:T(8,128)}, f32[4,128,256]{1,2,0:T(8,128)S(1)}, u32[]{:S(2)}) copy-start(f32[4,128,256]{1,2,0:T(8,128)S(1)} %get-tuple-element.5) | copy-start | bytes 1572868
  337.4 14.7 %copy-start.2 = (f32[4,64,256]{1,2,0:T(8,128)}, f32[4,64,256]{1,2,0:T(8,128)S(1)}, u32[]{:S(2)}) copy-start(f32[4,64,256]{1,2,0:T(8,128)S(1)} %get-tuple-element.19) | copy-start | bytes 786436
  358.6 9.1 %copy-start.3 = (f32[4,32,256]{1,2,0:T(8,128)}, f32[4,32,256]{1,2,0:T(8,128)S(1)}, u32[]{:S(2)}) copy-start(f32[4,32,256]{1,2,0:T(8,128)S(1)} %get-tuple-element.17) | copy-start | bytes 393220
  372.2 7.0 copy-start.5
  383.1 5.8 copy-start.6
  403.3 1.5 copy-start.9
  403.3 1.7 copy-start.18
  405.0 1.0 copy-start.7
  408.7 11.4 %copy-start.4 = (f32[4,32,256]{1,2,0:T(8,128)S(1)}, f32[4,32,256]{1,2,0:T(8,128)}, u32[]{:S(2)}) copy-start(f32[4,32,256]{1,2,0:T(8,128)} %copy-done.3) | copy-start | bytes 393220
  423.1 23.8 %copy-start.1 = (f32[4,128,256]{1,2,0:T(8,128)S(1)}, f32[4,128,256]{1,2,0:T(8,128)}, u32[]{:S(2)}) copy-start(f32[4,128,256]{1,2,0:T(8,128)} %copy-done) | copy-start | bytes 1572868
  463.7 4.3 copy-start.8
  496.5 5.5 copy-start.12
  496.5 5.5 copy-start.13
  502.1 4.7 copy-start.17
  506.8 15.3 %copy-start.10 = (f32[4,63,256]{1,2,0:T(8,128)S(1)}, f32[4,63,256]{1,2,0:T(8,128)}, u32[]{:S(2)}) copy-start(f32[4,63,256]{1,2,0:T(8,128)} %slice.259) | copy-start | bytes 774148
  506.8 15.3 %copy-start.11 = (f32[4,63,256]{1,2,0:T(8,128)S(1)}, f32[4,63,256]{1,2,0:T(8,128)}, u32[]{:S(2)}) copy-start(f32[4,63,256]{1,2,0:T(8,128)} %slice.210) | copy-start | bytes 774148
  522.5 9.1 %copy-start.20 = (f32[512,512]{1,0:T(8,128)S(1)}, f32[512,512]{1,0:T(8,128)}, u32[]{:S(2)}) copy-start(f32[512,512]{1,0:T(8,128)} %copy-done.19) | copy-start | bytes 3145732
  531.3 1.3 copy-start.31
  531.4 59.1 %copy-start.27 = (bf16[512,512]{1,0:T(8,128)(2,1)S(1)}, bf16[512,512]{1,0:T(8,128)(2,1)}, u32[]{:S(2)}) copy-start(bf16[512,512]{1,0:T(8,128)(2,1)} %fusion.29) | copy-start | bytes 1572868
  531.4 59.1 %copy-start.39 = (f32[1024]{0:T(1024)S(1)}, f32[1024]{0:T(1024)}, u32[]{:S(2)}) copy-start(f32[1024]{0:T(1024)} %param.30) | copy-start | bytes 12292
  532.5 57.9 %all-gather.27.cloned.1.call-start = ((), (), s32[]{:S(2)}) async-start(), calls=%async_computation.7 | async-start | bytes 1179648 | tf_op jit(solution)/shard_map/all_gather | solution.py:30
  533.3 81.7 %all-gather.29.cloned.1.call-start = ((), (), s32[]{:S(2)}) async-start(), calls=%async_computation.8 | async-start | bytes 2621440 | tf_op jit(solution)/shard_map/all_gather | solution.py:24
  549.5 44.3 %copy-start.23 = (f32[256,704]{0,1:T(8,128)S(1)}, f32[256,704]{0,1:T(8,128)}, u32[]{:S(2)}) copy-start(f32[256,704]{0,1:T(8,128)} %param.33) | copy-start | bytes 2162692
  549.6 44.3 %copy-start.24 = (f32[256,704]{0,1:T(8,128)S(1)}, f32[256,704]{0,1:T(8,128)}, u32[]{:S(2)}) copy-start(f32[256,704]{0,1:T(8,128)} %param.34) | copy-start | bytes 2162692
  593.6 1.3 copy-start.25
  593.6 116.5 %all-gather.31.cloned.1.call-start = ((), (), s32[]{:S(2)}) async-start(), calls=%async_computation.9 | async-start | bytes 6488064 | tf_op jit(solution)/shard_map/all_gather | solution.py:30
  594.9 115.2 %copy-start.38 = (f32[2048]{0:T(1024)S(1)}, f32[2048]{0:T(1024)}, u32[]{:S(2)}) copy-start(f32[2048]{0:T(1024)} %param.32) | copy-start | bytes 24580
  594.9 172.9 %all-gather.35.cloned.1.call-start = ((), (), s32[]{:S(2)}) async-start(), calls=%async_computation.11 | async-start | bytes 3244032 | tf_op jit(solution)/shard_map/all_gather | solution.py:30
  595.8 199.1 %all-gather.33.cloned.1.call-start = ((), (), s32[]{:S(2)}) async-start(), calls=%async_computation.10 | async-start | bytes 3604480 | tf_op jit(solution)/shard_map/all_gather | solution.py:40
  615.0 95.1 %copy-start.15 = (bf16[512,2048]{1,0:T(8,128)(2,1)S(1)}, bf16[512,2048]{1,0:T(8,128)(2,1)}, u32[]{:S(2)}) copy-start(bf16[512,2048]{1,0:T(8,128)(2,1)} %all-gather.29.cloned.1.call-done) | copy-start | bytes 6291460
  716.4 78.5 %copy-start.28 = (bf16[512,512]{1,0:T(8,128)(2,1)S(1)}, bf16[512,512]{1,0:T(8,128)(2,1)}, u32[]{:S(2)}) copy-start(bf16[512,512]{1,0:T(8,128)(2,1)} %fusion.30) | copy-start | bytes 1572868
  (4 other events, 4.0 us)
Sparse Core Ops, SparseCore 0:
  8.9 25.2 all-gather.12
  36.3 93.1 all-gather.14
  131.6 55.4 all-gather.18
  188.5 25.6 all-gather.16
  219.5 22.5 all-gather.20
  244.1 49.0 all-gather.22
  532.6 15.3 all-gather.24
  550.2 40.2 all-gather.26
  593.7 21.2 all-gather.28
  616.9 93.1 all-gather.30
  712.3 55.4 all-gather.34
  769.2 25.6 all-gather.32
where the time goes:
time: 815 us; the launch traced here: 807 us
  waiting for transfers between devices  510 us (63%)
  local copies, waits for them, and re-layouts  210 us (26%)
  other arithmetic  42.7 us (5%)
  matrix products  28.7 us (4%)
  between operations  14.5 us (2%)
    all_gather x6, waiting for transfers between devices, contract(): lax.all_gather(stacked.astype(jnp.bfloat16), 'fs', axis=0, tiled=True)  376 us
    slice x34, local copies, waits for them, and re-layouts, recurrent_mixer(): lax.associative_scan(combine, (jnp.exp(log_keep), inject), axis=1)  144 us
    all_gather x3, waiting for transfers between devices, widen(): return lax.all_gather(residual, 'tp', axis=1, tiled=True)  64.7 us
    all_gather x2, waiting for transfers between devices, feed_forward(): all_hidden = lax.all_gather(hidden, 'tp', axis=1, tiled=True)  54.2 us
    pad x12, local copies, waits for them, and re-layouts, recurrent_mixer(): lax.associative_scan(combine, (jnp.exp(log_keep), inject), axis=1)  50.5 us
    dot_general x6, matrix products, contract(): jnp.dot(operand, lax.all_gather(stacked.astype(jnp.bfloat16), 'fs', axis=...  28 us
  transfers between devices with their start and end apart: 12, of which 12 were waited for; matrix products, arithmetic and copies ran while one was open for 4% of the time, Pallas kernels for 0%

commit v1 on v0

--- a/solution.py
+++ b/solution.py
@@ -37,7 +37,7 @@
     products = contract(normed, jnp.concatenate((gate_matrix, up_matrix), axis=1))
     split_at = gate_matrix.shape[1]
     hidden = (jax.nn.silu(products[:, :split_at]) * products[:, split_at:]).astype(jnp.bfloat16)
-    all_hidden = lax.all_gather(hidden, "tp", axis=1, tiled=True)
+    all_hidden = jnp.concatenate(lax.all_gather(hidden, "tp"), axis=1)
     return (residual.astype(jnp.float32) + 0.5 * contract(all_hidden, down_matrix)).astype(
         jnp.bfloat16
     )

time: 815 us -> 832 us (1.021)
    all_gather x6, waiting for transfers between devices: 376 us -> 388 us  [contract(): lax.all_gather(stacked.astype(jnp.bfloat16), 'fs', axis=0, tiled=True)]
  transfers between devices with their start and end apart: 12 -> 12, of which waited for: 12 -> 12; matrix products, arithmetic and copies ran while one was open for 4% -> 3% of each run, Pallas kernels for 0% -> 0%
where the time goes in v1:
time: 832 us; the launch traced here: 824 us
  waiting for transfers between devices  518 us (62%)
  local copies, waits for them, and re-layouts  213 us (26%)
  other arithmetic  48.5 us (6%)
  matrix products  28.9 us (3%)
  between operations  14.5 us (2%)
    all_gather x6, waiting for transfers between devices, contract(): lax.all_gather(stacked.astype(jnp.bfloat16), 'fs', axis=0, tiled=True)  388 us
    slice x34, local copies, waits for them, and re-layouts, recurrent_mixer(): lax.associative_scan(combine, (jnp.exp(log_keep), inject), axis=1)  144 us
    all_gather x3, waiting for transfers between devices, widen(): return lax.all_gather(residual, 'tp', axis=1, tiled=True)  62.1 us
    all_gather x2, waiting for transfers between devices, feed_forward(): all_hidden = jnp.concatenate(lax.all_gather(hidden, 'tp'), axis=1)  51.9 us
    pad x12, local copies, waits for them, and re-layouts, recurrent_mixer(): lax.associative_scan(combine, (jnp.exp(log_keep), inject), axis=1)  50.4 us
    dot_general x6, matrix products, contract(): jnp.dot(operand, lax.all_gather(stacked.astype(jnp.bfloat16), 'fs', axis=...  28.2 us
  transfers between devices with their start and end apart: 12, of which 12 were waited for; matrix products, arithmetic and copies ran while one was open for 3% of the time, Pallas kernels for 0%

profile of v1, /device:TPU:0, one launch (start us, length us, event | category | flops | bytes accessed | tf_op | source)
XLA Modules:
  0.0 823.7 jit_solution(8854822473263605013)
XLA Ops:
  10.7 23.5 %all-gather.15.cloned.1.call-done = bf16[512,2048]{1,0:T(8,128)(2,1)} async-done(((bf16[512,512]{1,0:T(8,128)(2,1)}), bf16[512,2048]{1,0:T(8,128)(2,1)}) %all-gather.15.cloned.1.call-update) | async-done | bytes 2097168 | tf_op jit(solution)/shard_map/all_gather | solution.py:24
  36.3 93.1 %all-gather.17.cloned.1.call-done = bf16[2048,1408]{0,1:T(8,128)(2,1)} async-done(((bf16[256,1408]{0,1:T(8,128)(2,1)}), bf16[2048,1408]{0,1:T(8,128)(2,1)}) %all-gather.17.cloned.1.call-update) | async-done | bytes 5767184 | tf_op jit(solution)/shard_map/all_gather | solution.py:30
  129.4 6.5 fusion.16
  138.4 25.9 %all-gather.35.cloned.1.call-done = bf16[2048,704]{1,0:T(8,128)(2,1)} async-done(((bf16[512,704]{1,0:T(8,128)(2,1)}), bf16[2048,704]{1,0:T(8,128)(2,1)}) %all-gather.35.cloned.1.call-update) | async-done | bytes 2883600 | tf_op jit(solution)/shard_map/all_gather | solution.py:40
  164.4 3.2 copy.61
  167.5 56.2 %all-gather.19.cloned.1.call-done = bf16[2816,512]{1,0:T(8,128)(2,1)} async-done(((bf16[352,512]{1,0:T(8,128)(2,1)}), bf16[2816,512]{1,0:T(8,128)(2,1)}) %all-gather.19.cloned.1.call-update) | async-done | bytes 2883600 | tf_op jit(solution)/shard_map/all_gather | solution.py:30
  223.7 4.3 fusion.29
  230.9 18.5 %all-gather.21.cloned.1.call-done = bf16[512,2048]{1,0:T(8,128)(2,1)} async-done(((bf16[512,512]{1,0:T(8,128)(2,1)}), bf16[512,2048]{1,0:T(8,128)(2,1)}) %all-gather.21.cloned.1.call-update) | async-done | bytes 2097168 | tf_op jit(solution)/shard_map/all_gather | solution.py:24
  251.5 49.0 %all-gather.23.cloned.1.call-done = bf16[2048,512]{1,0:T(8,128)(2,1)} async-done(((bf16[256,512]{1,0:T(8,128)(2,1)}), bf16[2048,512]{1,0:T(8,128)(2,1)}) %all-gather.23.cloned.1.call-update) | async-done | bytes 2097168 | tf_op jit(solution)/shard_map/all_gather | solution.py:30
  300.5 3.5 fusion.14
  307.4 9.1 %slice.212 = f32[4,64,256]{1,2,0:T(8,128)S(1)} slice(f32[4,128,256]{1,2,0:T(8,128)S(1)} %get-tuple-element.6), slice={[0:4:1], [0:127:2], [0:256:1]} | slice | bytes 524288 | tf_op jit(solution)/shard_map/slice | solution.py:85
  316.5 9.1 %slice.213 = f32[4,64,256]{1,2,0:T(8,128)S(1)} slice(f32[4,128,256]{1,2,0:T(8,128)S(1)} %get-tuple-element.6), slice={[0:4:1], [1:128:2], [0:256:1]} | slice | bytes 524288 | tf_op jit(solution)/shard_map/slice | solution.py:85
  325.5 9.1 %slice.211 = f32[4,64,256]{1,2,0:T(8,128)S(1)} slice(f32[4,128,256]{1,2,0:T(8,128)S(1)} %get-tuple-element.5), slice={[0:4:1], [1:128:2], [0:256:1]} | slice | bytes 524288 | tf_op jit(solution)/shard_map/slice | solution.py:85
  334.6 9.5 %slice.215 = f32[4,64,256]{1,2,0:T(8,128)} slice(f32[4,128,256]{1,2,0:T(8,128)S(1)} %get-tuple-element.5), slice={[0:4:1], [0:127:2], [0:256:1]} | slice | bytes 524288 | tf_op jit(solution)/shard_map/slice | solution.py:85
  345.3 4.6 slice.218
  349.9 4.7 slice.219
  354.6 5.3 slice.217
  360.0 5.2 slice.221
  368.9 3.2 slice.225
  372.1 3.4 slice.223
  375.5 3.1 slice.227
  404.5 3.4 slice.241
  407.9 3.3 slice.245
  417.0 3.5 slice.234
  426.9 4.3 slice.222
  431.2 3.1 slice.255
  434.3 6.1 slice.216
  440.3 5.2 slice.257
  445.5 9.5 %slice.259 = f32[4,63,256]{1,2,0:T(8,128)} slice(f32[4,128,256]{1,2,0:T(8,128)S(1)} %get-tuple-element.6), slice={[0:4:1], [2:128:2], [0:256:1]} | slice | bytes 516096 | tf_op jit(solution)/shard_map/slice | solution.py:85
  455.0 9.9 %slice.210 = f32[4,63,256]{1,2,0:T(8,128)} slice(f32[4,128,256]{1,2,0:T(8,128)S(1)} %copy-done.1), slice={[0:4:1], [2:128:2], [0:256:1]} | slice | bytes 516096 | tf_op jit(solution)/shard_map/slice | solution.py:85
  471.9 4.3 pad.51
  495.8 2.9 pad.55
  499.5 3.7 pad.57
  505.5 3.6 pad.56
  510.3 4.5 pad.58
  514.8 4.6 pad.59
  520.3 9.8 %pad.61 = f32[4,128,256]{1,2,0:T(8,128)S(1)} pad(f32[4,64,256]{1,2,0:T(8,128)} %add.195, f32[]{:T(128)} %constant.10.clone.1), padding=0_0_0x1_0_1x0_0_0 | pad | bytes 786436 | tf_op jit(solution)/shard_map/pad | solution.py:85
  530.5 8.8 %pad.60 = f32[4,128,256]{1,2,0:T(8,128)S(1)} pad(f32[4,64,256]{1,2,0:T(8,128)S(1)} %pad_maximum_fusion.4, f32[]{:T(128)} %constant.10.clone.1), padding=0_0_0x0_1_1x0_0_0 | pad | bytes 786436 | tf_op jit(solution)/shard_map/pad | solution.py:85
  541.4 14.7 %all-gather.25.cloned.1.call-done = bf16[512,1024]{1,0:T(8,128)(2,1)} async-done(((bf16[512,256]{1,0:T(8,128)(2,1)}), bf16[512,1024]{1,0:T(8,128)(2,1)}) %all-gather.25.cloned.1.call-update) | async-done | bytes 1048592 | tf_op jit(solution)/shard_map/all_gather | solution.py:89
  557.6 40.9 %all-gather.27.cloned.1.call-done = bf16[1024,512]{1,0:T(8,128)(2,1)} async-done(((bf16[128,512]{1,0:T(8,128)(2,1)}), bf16[1024,512]{1,0:T(8,128)(2,1)}) %all-gather.27.cloned.1.call-update) | async-done | bytes 1048592 | tf_op jit(solution)/shard_map/all_gather | solution.py:30
  598.5 3.1 fusion.30
  603.0 20.0 %all-gather.29.cloned.1.call-done = bf16[512,2048]{1,0:T(8,128)(2,1)} async-done(((bf16[512,512]{1,0:T(8,128)(2,1)}), bf16[512,2048]{1,0:T(8,128)(2,1)}) %all-gather.29.cloned.1.call-update) | async-done | bytes 2097168 | tf_op jit(solution)/shard_map/all_gather | solution.py:24
  625.1 93.0 %all-gather.31.cloned.1.call-done = bf16[2048,1408]{0,1:T(8,128)(2,1)} async-done(((bf16[256,1408]{0,1:T(8,128)(2,1)}), bf16[2048,1408]{0,1:T(8,128)(2,1)}) %all-gather.31.cloned.1.call-update) | async-done | bytes 5767184 | tf_op jit(solution)/shard_map/all_gather | solution.py:30
  718.1 6.5 fusion.12
  727.0 26.0 %all-gather.37.cloned.1.call-done = bf16[2048,704]{1,0:T(8,128)(2,1)} async-done(((bf16[512,704]{1,0:T(8,128)(2,1)}), bf16[2048,704]{1,0:T(8,128)(2,1)}) %all-gather.37.cloned.1.call-update) | async-done | bytes 2883600 | tf_op jit(solution)/shard_map/all_gather | solution.py:40
  753.0 3.2 copy.83
  756.2 56.2 %all-gather.33.cloned.1.call-done = bf16[2816,512]{1,0:T(8,128)(2,1)} async-done(((bf16[352,512]{1,0:T(8,128)(2,1)}), bf16[2816,512]{1,0:T(8,128)(2,1)}) %all-gather.33.cloned.1.call-update) | async-done | bytes 2883600 | tf_op jit(solution)/shard_map/all_gather | solution.py:30
  812.4 4.3 fusion.28
  (181 shorter events, 101.1 us)
Async XLA Ops:
  6.5 27.7 %all-gather.15.cloned.1.call-start = ((), (), s32[]{:S(2)}) async-start(), calls=%async_computation | async-start | bytes 2621440 | tf_op jit(solution)/shard_map/all_gather | solution.py:24
  7.3 122.2 %all-gather.17.cloned.1.call-start = ((), (), s32[]{:S(2)}) async-start(), calls=%async_computation.1 | async-start | bytes 6488064 | tf_op jit(solution)/shard_map/all_gather | solution.py:30
  8.5 121.0 %copy-start.28 = (f32[2048]{0:T(1024)S(1)}, f32[2048]{0:T(1024)}, u32[]{:S(2)}) copy-start(f32[2048]{0:T(1024)} %param.19) | copy-start | bytes 24580
  10.6 153.7 %all-gather.35.cloned.1.call-start = ((), (), s32[]{:S(2)}) async-start(), calls=%async_computation.10 | async-start | bytes 3932160 | tf_op jit(solution)/shard_map/all_gather | solution.py:40
  135.9 1.6 copy-start.16
  137.5 86.2 %all-gather.19.cloned.1.call-start = ((), (), s32[]{:S(2)}) async-start(), calls=%async_computation.2 | async-start | bytes 3244032 | tf_op jit(solution)/shard_map/all_gather | solution.py:30
  138.4 111.0 %all-gather.21.cloned.1.call-start = ((), (), s32[]{:S(2)}) async-start(), calls=%async_computation.3 | async-start | bytes 2621440 | tf_op jit(solution)/shard_map/all_gather | solution.py:24
  164.3 59.4 %copy-start.20 = (bf16[512,512]{1,0:T(8,128)(2,1)S(1)}, bf16[512,512]{1,0:T(8,128)(2,1)}, u32[]{:S(2)}) copy-start(bf16[512,512]{1,0:T(8,128)(2,1)} %param.18) | copy-start | bytes 1572868
  223.7 7.1 copy-start.25
  223.7 7.2 copy-start.24
  228.0 72.5 %copy-start.29 = (f32[2048]{0:T(1024)S(1)}, f32[2048]{0:T(1024)}, u32[]{:S(2)}) copy-start(f32[2048]{0:T(1024)} %param.23) | copy-start | bytes 24580
  228.1 72.4 %all-gather.23.cloned.1.call-start = ((), (), s32[]{:S(2)}) async-start(), calls=%async_computation.4 | async-start | bytes 2359296 | tf_op jit(solution)/shard_map/all_gather | solution.py:30
  230.8 325.2 %all-gather.25.cloned.1.call-start = ((), (), s32[]{:S(2)}) async-start(), calls=%async_computation.5 | async-start | bytes 1310720 | tf_op jit(solution)/shard_map/all_gather | solution.py:89
  304.0 1.0 copy-start.14
  304.0 1.8 copy-start.26
  305.1 1.2 copy-start.27
  307.3 27.2 %copy-start = (f32[4,128,256]{1,2,0:T(8,128)}, f32[4,128,256]{1,2,0:T(8,128)S(1)}, u32[]{:S(2)}) copy-start(f32[4,128,256]{1,2,0:T(8,128)S(1)} %get-tuple-element.5) | copy-start | bytes 1572868
  345.3 14.7 %copy-start.2 = (f32[4,64,256]{1,2,0:T(8,128)}, f32[4,64,256]{1,2,0:T(8,128)S(1)}, u32[]{:S(2)}) copy-start(f32[4,64,256]{1,2,0:T(8,128)S(1)} %get-tuple-element.19) | copy-start | bytes 786436
  366.5 9.0 %copy-start.3 = (f32[4,32,256]{1,2,0:T(8,128)}, f32[4,32,256]{1,2,0:T(8,128)S(1)}, u32[]{:S(2)}) copy-start(f32[4,32,256]{1,2,0:T(8,128)S(1)} %get-tuple-element.17) | copy-start | bytes 393220
  380.0 7.0 copy-start.4
  390.9 5.8 copy-start.6
  411.2 3.2 copy-start.7
  416.1 6.3 copy-start.5
  426.9 28.1 %copy-start.1 = (f32[4,128,256]{1,2,0:T(8,128)S(1)}, f32[4,128,256]{1,2,0:T(8,128)}, u32[]{:S(2)}) copy-start(f32[4,128,256]{1,2,0:T(8,128)} %copy-done) | copy-start | bytes 1572868
  471.9 4.3 copy-start.8
  504.5 5.5 copy-start.11
  504.5 5.5 copy-start.12
  510.1 4.7 copy-start.13
  510.1 20.1 %copy-start.9 = (f32[4,63,256]{1,2,0:T(8,128)S(1)}, f32[4,63,256]{1,2,0:T(8,128)}, u32[]{:S(2)}) copy-start(f32[4,63,256]{1,2,0:T(8,128)} %slice.259) | copy-start | bytes 774148
  510.1 20.1 %copy-start.10 = (f32[4,63,256]{1,2,0:T(8,128)S(1)}, f32[4,63,256]{1,2,0:T(8,128)}, u32[]{:S(2)}) copy-start(f32[4,63,256]{1,2,0:T(8,128)} %slice.210) | copy-start | bytes 774148
  530.3 9.3 %copy-start.15 = (f32[512,512]{1,0:T(8,128)S(1)}, f32[512,512]{1,0:T(8,128)}, u32[]{:S(2)}) copy-start(f32[512,512]{1,0:T(8,128)} %copy-done.14) | copy-start | bytes 3145732
  530.5 10.1 %copy-start.23 = (f32[128,512]{1,0:T(8,128)S(1)}, f32[128,512]{1,0:T(8,128)}, u32[]{:S(2)}) copy-start(f32[128,512]{1,0:T(8,128)} %param.31) | copy-start | bytes 786436
  539.3 59.2 %copy-start.31 = (f32[1024]{0:T(1024)S(1)}, f32[1024]{0:T(1024)}, u32[]{:S(2)}) copy-start(f32[1024]{0:T(1024)} %param.30) | copy-start | bytes 12292
  539.4 59.1 %copy-start.21 = (bf16[512,512]{1,0:T(8,128)(2,1)S(1)}, bf16[512,512]{1,0:T(8,128)(2,1)}, u32[]{:S(2)}) copy-start(bf16[512,512]{1,0:T(8,128)(2,1)} %fusion.29) | copy-start | bytes 1572868
  540.5 57.9 %all-gather.27.cloned.1.call-start = ((), (), s32[]{:S(2)}) async-start(), calls=%async_computation.6 | async-start | bytes 1179648 | tf_op jit(solution)/shard_map/all_gather | solution.py:30
  541.3 60.5 %copy-start.17 = (f32[256,704]{0,1:T(8,128)S(1)}, f32[256,704]{0,1:T(8,128)}, u32[]{:S(2)}) copy-start(f32[256,704]{0,1:T(8,128)} %param.33) | copy-start | bytes 2162692
  541.3 81.7 %all-gather.29.cloned.1.call-start = ((), (), s32[]{:S(2)}) async-start(), calls=%async_computation.7 | async-start | bytes 2621440 | tf_op jit(solution)/shard_map/all_gather | solution.py:24
  557.6 44.3 %copy-start.18 = (f32[256,704]{0,1:T(8,128)S(1)}, f32[256,704]{0,1:T(8,128)}, u32[]{:S(2)}) copy-start(f32[256,704]{0,1:T(8,128)} %param.34) | copy-start | bytes 2162692
  601.6 116.5 %all-gather.31.cloned.1.call-start = ((), (), s32[]{:S(2)}) async-start(), calls=%async_computation.8 | async-start | bytes 6488064 | tf_op jit(solution)/shard_map/all_gather | solution.py:30
  601.9 116.2 %copy-start.30 = (f32[2048]{0:T(1024)S(1)}, f32[2048]{0:T(1024)}, u32[]{:S(2)}) copy-start(f32[2048]{0:T(1024)} %param.32) | copy-start | bytes 24580
  603.0 150.1 %all-gather.37.cloned.1.call-start = ((), (), s32[]{:S(2)}) async-start(), calls=%async_computation.11 | async-start | bytes 3932160 | tf_op jit(solution)/shard_map/all_gather | solution.py:40
  724.6 1.6 copy-start.19
  726.2 86.2 %all-gather.33.cloned.1.call-start = ((), (), s32[]{:S(2)}) async-start(), calls=%async_computation.9 | async-start | bytes 3244032 | tf_op jit(solution)/shard_map/all_gather | solution.py:30
  753.0 59.4 %copy-start.22 = (bf16[512,512]{1,0:T(8,128)(2,1)S(1)}, bf16[512,512]{1,0:T(8,128)(2,1)}, u32[]{:S(2)}) copy-start(bf16[512,512]{1,0:T(8,128)(2,1)} %fusion.30) | copy-start | bytes 1572868
Sparse Core Ops, SparseCore 0:
  8.9 25.2 all-gather.14
  36.3 93.1 all-gather.16
  137.6 26.6 all-gather.34
  166.4 57.2 all-gather.18
  228.2 21.1 all-gather.20
  251.4 49.0 all-gather.22
  540.6 15.3 all-gather.24
  558.2 40.2 all-gather.26
  601.7 21.2 all-gather.28
  624.9 93.1 all-gather.30
  726.3 26.6 all-gather.36
  755.1 57.2 all-gather.32
